TPU v7x, 32 devices: a whole 2x2x4 slice. The times are simulated.
32 devices in a mesh: sp: 8 (over z, x), tp: 4 (over y, core).
Axes of the slice: x: 2, y: 2, z: 4, core: 2. Of those that a mesh axis runs over, the one named last changes fastest.
Arguments:
- queries: bfloat16 [8192, 1536], P('sp', 'tp'), may hold values from -200 to 200
- key_heads: bfloat16 [8192, 512], P('sp', 'tp'), may hold values from -6 to 6
- projected_value_heads: bfloat16 [8192, 512], P('sp', 'tp'), may hold values from -5 to 5
- sink_logit_table: float32 [24], P('tp'), may hold values from 0 to 4
- out_weight: bfloat16 [1536, 3072], P('tp'), may hold values from -1.5 to 1.5
- residual: bfloat16 [8192, 3072], P('sp', 'tp'), may hold values from -16 to 16
- norm_gain: bfloat16 [3072], P('tp'), may hold values from 0.099609375 to 1.8984375
- up_weight: bfloat16 [3072, 12288], P('sp', 'tp'), may hold values from -0.109375 to 0.109375
- down_weight: bfloat16 [12288, 3072], P('tp', 'sp'), may hold values from -0.0546875 to 0.0546875
Outputs:
- result: bfloat16 [8192, 3072], P('sp', 'tp')
All inputs are finite; a program needn't handle non-finite values.
Results may differ from a plain program's by a relative error of at most 0.015.
Values may be sent and summed in bfloat16 or wider, within the bound.
No kernel may reach another device: no remote copies, remote signals or barrier semaphores. Data moves between devices by JAX's collectives and lax.ppermute only.
A program may use at most 128 MiB of HBM per device.

v0:
```python
import jax
import jax.numpy as jnp
from jax import lax
from jax.sharding import PartitionSpec as P

D = 3072
HEAD_SIZE = 64
WINDOW_SPAN = 128
epsilon = 1e-06


def shifted(block, axis, distance):
    devices = range(lax.axis_size(axis))
    route = [(i - distance, i) for i in devices if i - distance in devices]
    return lax.ppermute(block, axis, route)


def attend(queries, key_heads, projected_value_heads, sink_logit_table, previous, offset):
    row_count = queries.shape[0]
    kv_cols = key_heads.shape[1]
    kv_local = kv_cols // HEAD_SIZE
    group_count = queries.shape[1] // kv_cols
    block_count = row_count // WINDOW_SPAN
    extended_keys = jnp.concatenate([previous[:, :kv_cols], key_heads], axis=0)
    extended_values = jnp.concatenate([previous[:, kv_cols:], projected_value_heads], axis=0)

    def banded(source_rows):
        shaped = source_rows.reshape(block_count + 1, WINDOW_SPAN, kv_local, HEAD_SIZE)
        return jnp.concatenate([shaped[:-1], shaped[1:]], axis=1)

    key_band = banded(extended_keys)
    value_band = banded(extended_values)
    query_block_list = queries.reshape(block_count, WINDOW_SPAN, kv_local, group_count, HEAD_SIZE)
    scores = jnp.einsum(
        "nqkgd,nskd->nkgqs", query_block_list, key_band, preferred_element_type=jnp.float32
    ) * HEAD_SIZE ** (-0.5)
    within = jnp.arange(WINDOW_SPAN)[:, None]
    column = jnp.arange(2 * WINDOW_SPAN)[None, :]
    distance = WINDOW_SPAN + within - column
    valid = (distance >= 0) & (distance < WINDOW_SPAN)
    key_pos = (
        offset
        + jnp.arange(block_count)[:, None] * WINDOW_SPAN
        + jnp.arange(2 * WINDOW_SPAN)[None, :]
        - WINDOW_SPAN
    )
    allowed = valid[None] & (key_pos >= 0)[:, None, :]
    allowed = allowed[:, None, None]
    head_sink_logit = sink_logit_table.reshape(kv_local, group_count)[None, :, :, None, None]
    masked = jnp.where(allowed, scores, -1e30)
    ceiling = jnp.maximum(jnp.max(masked, axis=-1, keepdims=True), head_sink_logit)
    powers = jnp.where(allowed, jnp.exp(masked - ceiling), 0.0)
    denom = jnp.sum(powers, axis=-1, keepdims=True) + jnp.exp(head_sink_logit - ceiling)
    probs = (powers / denom).astype(jnp.bfloat16)
    output = jnp.einsum("nkgqs,nskd->nqkgd", probs, value_band, preferred_element_type=jnp.float32)
    return output.astype(jnp.bfloat16).reshape(row_count, queries.shape[1])


def rounded(values):
    return lax.optimization_barrier(values.astype(jnp.bfloat16)).astype(jnp.float32)


def body(
    queries,
    key_heads,
    projected_value_heads,
    sink_logit_table,
    out_weight,
    residual,
    norm_gain,
    up_weight,
    down_weight,
):
    row_count = queries.shape[0]
    offset = lax.axis_index("sp") * row_count
    tail = jnp.concatenate(
        [key_heads[row_count - WINDOW_SPAN :], projected_value_heads[row_count - WINDOW_SPAN :]],
        axis=1,
    )
    previous = shifted(tail, "sp", 1)
    attended = attend(queries, key_heads, projected_value_heads, sink_logit_table, previous, offset)
    partial_value = rounded(jnp.dot(attended, out_weight, preferred_element_type=jnp.float32))
    mixed_sum = lax.psum_scatter(
        partial_value.astype(jnp.bfloat16), "tp", scatter_dimension=1, tiled=True
    ).astype(jnp.float32)
    stream = rounded(residual.astype(jnp.float32) + mixed_sum)
    squares = lax.psum(jnp.sum(stream * stream, axis=1, keepdims=True), "tp")
    normed = (stream * lax.rsqrt(squares / D + epsilon) * norm_gain.astype(jnp.float32)).astype(
        jnp.bfloat16
    )
    normed_whole = lax.all_gather(normed, "tp", axis=1, tiled=True)
    hidden_pre = jnp.dot(
        normed_whole,
        lax.all_gather(up_weight, "sp", axis=0, tiled=True),
        preferred_element_type=jnp.float32,
    )
    activated = jnp.square(jax.nn.relu(hidden_pre)).astype(jnp.bfloat16)
    terms = jnp.dot(
        activated,
        lax.all_gather(down_weight, "sp", axis=1, tiled=True),
        preferred_element_type=jnp.float32,
    )
    branch_sum = lax.psum_scatter(
        rounded(terms).astype(jnp.bfloat16), "tp", scatter_dimension=1, tiled=True
    ).astype(jnp.float32)
    return (stream + branch_sum).astype(jnp.bfloat16)


def solution(mesh):
    return jax.shard_map(
        body,
        mesh=mesh,
        in_specs=(
            P("sp", "tp"),
            P("sp", "tp"),
            P("sp", "tp"),
            P("tp"),
            P("tp", None),
            P("sp", "tp"),
            P("tp"),
            P("sp", "tp"),
            P("tp", "sp"),
        ),
        out_specs=P("sp", "tp"),
        check_vma=False,
    )
```

profile of v0, /device:TPU:0, one launch (start us, length us, event | category | flops | bytes accessed | tf_op | source)
XLA Modules:
  0.0 985.8 jit_solution(6724844009850247608)
XLA Ops:
  6.5 0.0 copy-start
  6.5 0.0 copy-start.4
  6.5 0.0 reduce-scatter.3.cloned.1.call-start
  6.5 0.9 slice.32
  7.5 0.8 slice.33
  8.2 4.9 collective-permute-start
  13.2 0.1 add_compare_fusion
  13.3 1.0 broadcast_and_fusion
  14.3 2.0 reshape.91
  16.3 2.0 reshape.89
  18.3 1.4 copy.20
  19.7 1.1 copy.35
  20.8 1.9 copy.19
  22.7 0.7 max.26
  23.4 1.9 copy.15
  25.3 0.0 collective-permute-done
  25.3 0.0 copy-done.4
  25.3 1.7 pad_maximum_fusion
  27.0 1.2 reshape.90
  28.2 1.0 copy.18
  29.1 0.0 copy-start.5
  29.2 2.5 fusion
  31.6 0.0 copy-start.3
  31.7 0.1 broadcast_maximum_fusion
  31.7 2.6 copy-done.3
  34.3 2.8 fusion.1
  37.1 0.1 exponential_add_fusion
  37.2 0.2 reshape.88
  37.5 0.4 copy.14
  37.8 0.0 copy-done.5
  37.9 4.9 fusion.8
  42.7 0.5 copy.23
  43.3 0.0 copy-done
  43.3 0.0 copy-start.6
  43.3 5.4 convolution_convert_fusion.1
  48.7 0.0 reduce-scatter.3.cloned.1.call-update
  48.7 0.0 all-gather.4.cloned.1.call-start
  48.8 0.0 copy-done.6
  48.8 58.3 %reduce-scatter.3.cloned.1.call-done = bf16[1024,768]{1,0:T(8,128)(2,1)} async-done(((bf16[1024,3072]{1,0:T(8,128)(2,1)}), bf16[1024,768]{1,0:T(8,128)(2,1)}) %reduce-scatter.3.cloned.1.call-update) | async-done | bytes 1572880 | tf_op jit(solution)/shard_map/reduce_scatter | solution.py:83
  107.1 2.3 add_convert_fusion
  109.3 0.0 copy-start.2
  109.3 0.4 fusion.2
  109.7 5.8 psum.7
  115.5 1.5 fusion.4
  117.0 0.0 all-gather.4.cloned.1.call-update
  117.1 0.0 all-gather.6.cloned.1.call-start
  117.1 0.7 all-gather.6.cloned.1.call-update
  117.8 0.0 all-gather.8.cloned.1.call-start
  117.9 0.5 all-gather.8.cloned.1.call-update
  118.4 0.2 reduce-scatter.5.cloned.1.call-start
  118.6 45.6 %all-gather.4.cloned.1.call-done = bf16[1024,3072]{1,0:T(8,128)(2,1)} async-done(((bf16[1024,768]{1,0:T(8,128)(2,1)}), bf16[1024,3072]{1,0:T(8,128)(2,1)}) %all-gather.4.cloned.1.call-update) | async-done | bytes 6291472 | tf_op jit(solution)/shard_map/all_gather | solution.py:91
  164.2 364.0 %all-gather.6.cloned.1.call-done = bf16[3072,3072]{1,0:T(8,128)(2,1)} async-done(((bf16[384,3072]{1,0:T(8,128)(2,1)}), bf16[3072,3072]{1,0:T(8,128)(2,1)}) %all-gather.6.cloned.1.call-update) | async-done | bytes 18874384 | tf_op jit(solution)/shard_map/all_gather | solution.py:94
  528.2 25.8 %multiply_convert_fusion.clone.4 = bf16[1024,3072]{1,0:T(8,128)(2,1)} fusion(bf16[1024,3072]{1,0:T(8,128)(2,1)} %all-gather.4.cloned.1.call-done, bf16[3072,3072]{1,0:T(8,128)(2,1)} %all-gather.6.cloned.1.call-done), kind=kOutput, calls=%fused_computation.clone.clone.clone.1 | convolution fusion | flops 19336790016 | bytes 31457280 | tf_op jit(solution)/shard_map/dot_general | solution.py:92
  553.9 0.0 copy-done.2
  553.9 338.0 %all-gather.8.cloned.1.call-done = bf16[3072,3072]{1,0:T(8,128)(2,1)} async-done(((bf16[3072,384]{1,0:T(8,128)(2,1)}), bf16[3072,3072]{1,0:T(8,128)(2,1)}) %all-gather.8.cloned.1.call-update) | async-done | bytes 18874384 | tf_op jit(solution)/shard_map/all_gather | solution.py:100
  892.0 0.0 copy-start.1
  892.0 25.8 %convolution_convert_fusion = bf16[1024,3072]{1,0:T(8,128)(2,1)} fusion(bf16[3072,3072]{1,0:T(8,128)(2,1)} %all-gather.8.cloned.1.call-done, bf16[1024,3072]{1,0:T(8,128)(2,1)} %multiply_convert_fusion.clone.4), kind=kOutput, calls=%fused_computation.4 | convolution fusion | flops 19330498560 | bytes 31457280 | tf_op jit(solution)/shard_map/dot_general | solution.py:98
  917.8 0.0 reduce-scatter.5.cloned.1.call-update
  917.9 58.0 %reduce-scatter.5.cloned.1.call-done = bf16[1024,768]{1,0:T(8,128)(2,1)} async-done(((bf16[1024,3072]{1,0:T(8,128)(2,1)}), bf16[1024,768]{1,0:T(8,128)(2,1)}) %reduce-scatter.5.cloned.1.call-update) | async-done | bytes 1572880 | tf_op jit(solution)/shard_map/reduce_scatter | solution.py:103
  975.9 3.4 fusion.5
  979.3 0.0 copy-done.1
  (7 shorter events, 0.1 us)
Async XLA Ops:
  6.5 36.7 %copy-start = (bf16[384,3072]{1,0:T(8,128)(2,1)S(1)}, bf16[384,3072]{1,0:T(8,128)(2,1)}, u32[]{:S(2)}) copy-start(bf16[384,3072]{1,0:T(8,128)(2,1)} %param.13) | copy-start | bytes 7077892
  6.5 18.8 %copy-start.4 = (bf16[1024,128]{1,0:T(8,128)(2,1)S(1)}, bf16[1024,128]{1,0:T(8,128)(2,1)}, u32[]{:S(2)}) copy-start(bf16[1024,128]{1,0:T(8,128)(2,1)} %param.10) | copy-start | bytes 786436
  6.5 100.5 %reduce-scatter.3.cloned.1.call-start = ((), (), s32[]{:S(2)}) async-start(), calls=%async_computation.2 | async-start | bytes 7864320 | tf_op jit(solution)/shard_map/reduce_scatter | solution.py:83
  8.2 17.1 %collective-permute-start = (bf16[128,256]{1,0:T(8,128)(2,1)S(1)}, bf16[128,256]{1,0:T(8,128)(2,1)S(1)}, u32[]{:S(2)}, u32[]{:S(2)}) collective-permute-start(bf16[128,256]{1,0:T(8,128)(2,1)S(1)} %pad_maximum_fusion.2), channel_id=1, source_target_pairs={{0,4},{4,8},{8,12},{12,16},{16,20},{20,24},{24,28},{1,5},{5,9},{9,... | collective-permute-start | bytes 196616 | tf_op jit(solution)/shard_map/ppermute | solution.py:15
  29.1 8.7 copy-start.5
  31.6 2.7 copy-start.3
  43.3 5.5 copy-start.6
  48.7 115.5 %all-gather.4.cloned.1.call-start = ((), (), s32[]{:S(2)}) async-start(), calls=%async_computation.3 | async-start | bytes 7864320 | tf_op jit(solution)/shard_map/all_gather | solution.py:91
  109.3 444.6 %copy-start.2 = (bf16[1024,768]{1,0:T(8,128)(2,1)}, bf16[1024,768]{1,0:T(8,128)(2,1)S(1)}, u32[]{:S(2)}) copy-start(bf16[1024,768]{1,0:T(8,128)(2,1)S(1)} %add_convert_fusion) | copy-start | bytes 4718596
  117.1 411.1 %all-gather.6.cloned.1.call-start = ((), (), s32[]{:S(2)}) async-start(), calls=%async_computation.4 | async-start | bytes 21233664 | tf_op jit(solution)/shard_map/all_gather | solution.py:94
  117.8 774.2 %all-gather.8.cloned.1.call-start = ((), (), s32[]{:S(2)}) async-start(), calls=%async_computation.5 | async-start | bytes 21233664 | tf_op jit(solution)/shard_map/all_gather | solution.py:100
  118.4 857.5 %reduce-scatter.5.cloned.1.call-start = ((), (), s32[]{:S(2)}) async-start(), calls=%async_computation.6 | async-start | bytes 7864320 | tf_op jit(solution)/shard_map/reduce_scatter | solution.py:103
  892.0 87.3 %copy-start.1 = (bf16[384,3072]{1,0:T(8,128)(2,1)S(1)}, bf16[384,3072]{1,0:T(8,128)(2,1)}, u32[]{:S(2)}) copy-start(bf16[384,3072]{1,0:T(8,128)(2,1)} %param.13) | copy-start | bytes 7077892
Sparse Core Ops, SparseCore 0:
  48.8 58.1 reduce-scatter.2
  117.2 46.9 all-gather.3
  165.8 362.3 all-gather.5
  529.6 362.3 all-gather.7
  918.0 57.8 reduce-scatter.4
where the time goes:
time: 986 us
  waiting for transfers between devices  865 us (88%)
  matrix products  64.4 us (7%)
  local copies, waits for them, and re-layouts  18.5 us (2%)
  other arithmetic  13.4 us (1%)
  between operations  13.3 us (1%)
    all_gather x1, waiting for transfers between devices, body(): lax.all_gather(up_weight, 'sp', axis=0, tiled=True)  364 us
    all_gather x1, waiting for transfers between devices, body(): lax.all_gather(down_weight, 'sp', axis=1, tiled=True)  338 us
    reduce_scatter x1, waiting for transfers between devices, body(): lax.psum_scatter(partial_value.astype(jnp.bfloat16), 'tp', scatter_dimens...  58.3 us
    reduce_scatter x1, waiting for transfers between devices, body(): lax.psum_scatter(rounded(terms).astype(jnp.bfloat16), 'tp', scatter_dimen...  58 us
    all_gather x1, waiting for transfers between devices, body(): normed_whole = lax.all_gather(normed, 'tp', axis=1, tiled=True)  45.6 us
    dot_general x1, matrix products, body(): jnp.dot(activated, lax.all_gather(down_weight, 'sp', axis=1, tiled=True),...  25.8 us
    dot_general x1, matrix products, body(): jnp.dot(normed_whole, lax.all_gather(up_weight, 'sp', axis=0, tiled=True)...  25.8 us
  transfers between devices with their start and end apart: 6, of which 5 were waited for; matrix products, arithmetic and copies ran while one was open for 4% of the time, Pallas kernels for 0%

commit v1 on v0

--- a/solution.py
+++ b/solution.py
@@ -1,3 +1,4 @@
+import functools
 import jax
 import jax.numpy as jnp
 from jax import lax
@@ -7,6 +8,14 @@
 HEAD_SIZE = 64
 WINDOW_SPAN = 128
 epsilon = 1e-06
+
+
+def load_cards(raw, axis_id, array_axis):
+    near = lax.all_gather(raw, axis_name=axis_id)
+    return jnp.concatenate(near, array_axis)
+
+
+windows_resolve = functools.partial(load_cards, axis_id="sp", array_axis=1)
 
 
 def shifted(block, axis, distance):
@@ -95,11 +104,7 @@
         preferred_element_type=jnp.float32,
     )
     activated = jnp.square(jax.nn.relu(hidden_pre)).astype(jnp.bfloat16)
-    terms = jnp.dot(
-        activated,
-        lax.all_gather(down_weight, "sp", axis=1, tiled=True),
-        preferred_element_type=jnp.float32,
-    )
+    terms = jnp.dot(activated, windows_resolve(down_weight), preferred_element_type=jnp.float32)
     branch_sum = lax.psum_scatter(
         rounded(terms).astype(jnp.bfloat16), "tp", scatter_dimension=1, tiled=True
     ).astype(jnp.float32)

time: 986 us -> 946 us (0.959)
  waiting for transfers between devices: 865 us -> 799 us
  local copies, waits for them, and re-layouts: 18.5 us -> 43.3 us
    all_gather x1, waiting for transfers between devices: 338 us -> 295 us  [load_cards(): near = lax.all_gather(raw, axis_name=axis_id)]
    reshape x0 -> x1, local copies, waits for them, and re-layouts: none -> 24.8 us  [load_cards(): return jnp.concatenate(near, array_axis)]
    all_gather x1, waiting for transfers between devices: 45.6 us -> 22.9 us  [body(): normed_whole = lax.all_gather(normed, 'tp', axis=1, tiled=True)]
where the time goes in v1:
time: 946 us; the launch traced here: 945 us
  waiting for transfers between devices  799 us (84%)
  matrix products  63 us (7%)
  local copies, waits for them, and re-layouts  43.3 us (5%)
  between operations  15.2 us (2%)
  other arithmetic  13.5 us (1%)
    all_gather x1, waiting for transfers between devices, body(): lax.all_gather(up_weight, 'sp', axis=0, tiled=True)  364 us
    all_gather x1, waiting for transfers between devices, load_cards(): near = lax.all_gather(raw, axis_name=axis_id)  295 us
    reduce_scatter x1, waiting for transfers between devices, body(): lax.psum_scatter(rounded(terms).astype(jnp.bfloat16), 'tp', scatter_dimen...  58 us
    reduce_scatter x1, waiting for transfers between devices, body(): lax.psum_scatter(partial_value.astype(jnp.bfloat16), 'tp', scatter_dimens...  57.7 us
    dot_general x1, matrix products, body(): jnp.dot(normed_whole, lax.all_gather(up_weight, 'sp', axis=0, tiled=True)...  25.7 us
    reshape x1, local copies, waits for them, and re-layouts, load_cards(): return jnp.concatenate(near, array_axis)  24.8 us
    dot_general x1, matrix products, body(): jnp.dot(activated, windows_resolve(down_weight), preferred_element_type=j...  24.5 us
    all_gather x1, waiting for transfers between devices, body(): normed_whole = lax.all_gather(normed, 'tp', axis=1, tiled=True)  22.9 us
  transfers between devices with their start and end apart: 6, of which 5 were waited for; matrix products, arithmetic and copies ran while one was open for 4% of the time, Pallas kernels for 0%

profile of v1, /device:TPU:0, one launch (start us, length us, event | category | flops | bytes accessed | tf_op | source)
XLA Modules:
  0.0 944.9 jit_solution(15052837907160689385)
XLA Ops:
  7.4 0.0 copy-start
  7.4 0.0 copy-start.5
  7.4 0.0 reduce-scatter.3.cloned.1.call-start
  7.4 0.9 slice.32
  8.3 0.8 slice.33
  9.1 4.9 collective-permute-start
  14.0 0.1 add_compare_fusion
  14.1 1.0 broadcast_and_fusion
  15.1 2.0 reshape.100
  17.1 2.0 reshape.98
  19.1 1.4 copy.32
  20.5 1.1 copy.48
  21.6 1.9 copy.31
  23.5 0.7 max.26
  24.2 1.9 copy.27
  26.1 0.0 collective-permute-done
  26.1 0.0 copy-done.5
  26.1 1.7 pad_maximum_fusion
  27.8 1.2 reshape.99
  29.0 1.0 copy.30
  29.9 0.0 copy-start.6
  29.9 2.5 fusion
  32.4 0.0 copy-start.4
  32.5 0.1 broadcast_maximum_fusion
  32.5 2.6 copy-done.4
  35.1 2.8 fusion.1
  37.9 0.1 exponential_add_fusion
  38.0 0.2 reshape.97
  38.3 0.4 copy.26
  38.6 0.0 copy-done.6
  38.6 4.9 fusion.8
  43.5 0.5 copy.35
  44.0 0.0 copy-done
  44.1 5.4 convolution_convert_fusion.1
  49.4 0.0 copy-start.7
  49.4 0.0 reduce-scatter.3.cloned.1.call-update
  49.5 0.0 all-gather.9.cloned.1.call-start
  49.5 0.5 all-gather.9.cloned.1.call-update
  50.0 0.0 all-gather.5.cloned.1.call-start
  50.1 0.0 copy-done.7
  50.1 57.7 %reduce-scatter.3.cloned.1.call-done = bf16[1024,768]{1,0:T(8,128)(2,1)} async-done(((bf16[1024,3072]{1,0:T(8,128)(2,1)}), bf16[1024,768]{1,0:T(8,128)(2,1)}) %reduce-scatter.3.cloned.1.call-update) | async-done | bytes 1572880 | tf_op jit(solution)/shard_map/reduce_scatter | solution.py:92
  107.8 2.3 add_convert_fusion
  110.1 0.0 copy-start.2
  110.1 0.4 fusion.2
  110.5 6.1 psum.7
  116.6 1.6 fusion.4
  118.2 0.0 all-gather.5.cloned.1.call-update
  118.2 0.0 all-gather.7.cloned.1.call-start
  118.2 0.5 all-gather.7.cloned.1.call-update
  118.8 0.2 reduce-scatter.5.cloned.1.call-start
  119.0 295.2 %all-gather.9.cloned.1.call-done = bf16[24576,384]{1,0:T(8,128)(2,1)} async-done(((bf16[3072,384]{1,0:T(8,128)(2,1)}), bf16[24576,384]{1,0:T(8,128)(2,1)}) %all-gather.9.cloned.1.call-update) | async-done | bytes 18874384 | tf_op jit(solution)/shard_map/all_gather | solution.py:14
  414.2 24.8 %copy.36 = bf16[3072,8,384]{0,2,1:T(8,128)(2,1)} copy(bf16[3072,8,384]{2,0,1:T(8,128)(2,1)} %bitcast.59) | data formatting | bytes 37748736 | tf_op jit(solution)/shard_map/reshape | solution.py:15
  439.0 0.0 copy-done.2
  439.0 22.9 %all-gather.5.cloned.1.call-done = bf16[1024,3072]{1,0:T(8,128)(2,1)} async-done(((bf16[1024,768]{1,0:T(8,128)(2,1)}), bf16[1024,3072]{1,0:T(8,128)(2,1)}) %all-gather.5.cloned.1.call-update) | async-done | bytes 6291472 | tf_op jit(solution)/shard_map/all_gather | solution.py:100
  461.9 363.8 %all-gather.7.cloned.1.call-done = bf16[3072,3072]{1,0:T(8,128)(2,1)} async-done(((bf16[384,3072]{1,0:T(8,128)(2,1)}), bf16[3072,3072]{1,0:T(8,128)(2,1)}) %all-gather.7.cloned.1.call-update) | async-done | bytes 18874384 | tf_op jit(solution)/shard_map/all_gather | solution.py:103
  825.7 0.0 copy-start.3
  825.7 25.7 %multiply_convert_fusion.clone.4 = bf16[1024,3072]{1,0:T(8,128)(2,1)} fusion(bf16[1024,3072]{1,0:T(8,128)(2,1)} %all-gather.5.cloned.1.call-done, bf16[3072,3072]{1,0:T(8,128)(2,1)} %all-gather.7.cloned.1.call-done), kind=kOutput, calls=%fused_computation.clone.clone.clone.1 | convolution fusion | flops 19336790016 | bytes 31457280 | tf_op jit(solution)/shard_map/dot_general | solution.py:101
  851.4 0.0 copy-done.3
  851.4 0.0 copy-start.1
  851.4 24.5 %convolution_convert_fusion = bf16[1024,3072]{1,0:T(8,128)(2,1)} fusion(bf16[3072,3072]{0,1:T(8,128)(2,1)S(1)} %bitcast.60, bf16[1024,3072]{1,0:T(8,128)(2,1)} %multiply_convert_fusion.clone.4), kind=kOutput, calls=%fused_computation.4 | convolution fusion | flops 19330498560 | bytes 31457280 | tf_op jit(solution)/shard_map/dot_general | solution.py:107
  875.9 0.0 reduce-scatter.5.cloned.1.call-update
  876.0 58.0 %reduce-scatter.5.cloned.1.call-done = bf16[1024,768]{1,0:T(8,128)(2,1)} async-done(((bf16[1024,3072]{1,0:T(8,128)(2,1)}), bf16[1024,768]{1,0:T(8,128)(2,1)}) %reduce-scatter.5.cloned.1.call-update) | async-done | bytes 1572880 | tf_op jit(solution)/shard_map/reduce_scatter | solution.py:108
  933.9 3.4 fusion.5
  937.4 0.0 copy-done.1
  (7 shorter events, 0.1 us)
Async XLA Ops:
  7.4 36.7 %copy-start = (bf16[384,3072]{1,0:T(8,128)(2,1)S(1)}, bf16[384,3072]{1,0:T(8,128)(2,1)}, u32[]{:S(2)}) copy-start(bf16[384,3072]{1,0:T(8,128)(2,1)} %param.13) | copy-start | bytes 7077892
  7.4 18.7 %copy-start.5 = (bf16[1024,128]{1,0:T(8,128)(2,1)S(1)}, bf16[1024,128]{1,0:T(8,128)(2,1)}, u32[]{:S(2)}) copy-start(bf16[1024,128]{1,0:T(8,128)(2,1)} %param.10) | copy-start | bytes 786436
  7.4 100.4 %reduce-scatter.3.cloned.1.call-start = ((), (), s32[]{:S(2)}) async-start(), calls=%async_computation.2 | async-start | bytes 7864320 | tf_op jit(solution)/shard_map/reduce_scatter | solution.py:92
  9.1 17.0 %collective-permute-start = (bf16[128,256]{1,0:T(8,128)(2,1)S(1)}, bf16[128,256]{1,0:T(8,128)(2,1)S(1)}, u32[]{:S(2)}, u32[]{:S(2)}) collective-permute-start(bf16[128,256]{1,0:T(8,128)(2,1)S(1)} %pad_maximum_fusion.2), channel_id=1, source_target_pairs={{0,4},{4,8},{8,12},{12,16},{16,20},{20,24},{24,28},{1,5},{5,9},{9,... | collective-permute-start | bytes 196616 | tf_op jit(solution)/shard_map/ppermute | solution.py:24
  29.9 8.7 copy-start.6
  32.4 2.7 copy-start.4
  49.4 0.7 copy-start.7
  49.5 364.7 %all-gather.9.cloned.1.call-start = ((), (), s32[]{:S(2)}) async-start(), calls=%async_computation.6 | async-start | bytes 21233664 | tf_op jit(solution)/shard_map/all_gather | solution.py:14
  50.0 411.8 %all-gather.5.cloned.1.call-start = ((), (), s32[]{:S(2)}) async-start(), calls=%async_computation.3 | async-start | bytes 7864320 | tf_op jit(solution)/shard_map/all_gather | solution.py:100
  110.1 328.9 %copy-start.2 = (bf16[1024,768]{1,0:T(8,128)(2,1)}, bf16[1024,768]{1,0:T(8,128)(2,1)S(1)}, u32[]{:S(2)}) copy-start(bf16[1024,768]{1,0:T(8,128)(2,1)S(1)} %add_convert_fusion) | copy-start | bytes 4718596
  118.2 707.5 %all-gather.7.cloned.1.call-start = ((), (), s32[]{:S(2)}) async-start(), calls=%async_computation.4 | async-start | bytes 21233664 | tf_op jit(solution)/shard_map/all_gather | solution.py:103
  118.8 815.2 %reduce-scatter.5.cloned.1.call-start = ((), (), s32[]{:S(2)}) async-start(), calls=%async_computation.5 | async-start | bytes 7864320 | tf_op jit(solution)/shard_map/reduce_scatter | solution.py:108
  825.7 25.7 %copy-start.3 = (bf16[3072,8,384]{0,2,1:T(8,128)(2,1)S(1)}, bf16[3072,8,384]{0,2,1:T(8,128)(2,1)}, u32[]{:S(2)}) copy-start(bf16[3072,8,384]{0,2,1:T(8,128)(2,1)} %copy.36) | copy-start | bytes 56623108
  851.4 86.0 %copy-start.1 = (bf16[384,3072]{1,0:T(8,128)(2,1)S(1)}, bf16[384,3072]{1,0:T(8,128)(2,1)}, u32[]{:S(2)}) copy-start(bf16[384,3072]{1,0:T(8,128)(2,1)} %param.13) | copy-start | bytes 7077892
Sparse Core Ops, SparseCore 0:
  49.6 58.1 reduce-scatter.2
  876.1 57.8 reduce-scatter.4
Sparse Core Ops, SparseCore 1:
  51.5 362.7 all-gather.8
  415.6 46.2 all-gather.4
  463.3 362.3 all-gather.6
